TPU v7x, 128 devices: a whole 4x4x4 slice. The times are simulated.
128 devices in a mesh: ep: 64 (over z, y, x), tp: 2 (over core).
Axes of the slice: x: 4, y: 4, z: 4, core: 2. Of those that a mesh axis runs over, the one named last changes fastest.
Arguments:
- tokens: bfloat16 [4096, 2048], P('ep', 'tp'), may hold values from -6 to 6
- sequence_state_real: float32 [4096, 128, 64], P('ep', 'tp'), may hold values from -4 to 4
- sequence_state_imaginary: float32 [4096, 128, 64], P('ep', 'tp'), may hold values from -4 to 4
- mixer_norm_gain: float32 [2048], replicated, may hold values from 0.1 to 1.9
- expert_norm_gain: float32 [2048], replicated, may hold values from 0.1 to 1.9
- rate: float32 [128, 64], P('tp'), may hold values from 0.1 to 4
- freq: float32 [128, 64], P('tp'), may hold values from -3 to 3
- log_group_step: float32 [128], P('tp'), may hold values from -3 to 0
- input_map_real: float32 [128, 64, 16], P('tp'), may hold values from -1 to 1
- input_map_imaginary: float32 [128, 64, 16], P('tp'), may hold values from -1 to 1
- output_map_real: float32 [128, 16, 64], P('tp'), may hold values from -0.75 to 0.75
- output_map_imaginary: float32 [128, 16, 64], P('tp'), may hold values from -0.75 to 0.75
- skip: float32 [2048], P('tp'), may hold values from -4 to 4
- mixer_value_weight: bfloat16 [2048, 2048], P('tp'), may hold values from -0.125 to 0.125
- mixer_gate_weight: bfloat16 [2048, 2048], P('tp'), may hold values from -0.125 to 0.125
- group_router_weight: bfloat16 [2048, 4], replicated, may hold values from -0.125 to 0.125
- expert_router_weight: bfloat16 [2048, 64], replicated, may hold values from -0.125 to 0.125
- dense_blend_weight: float32 [2048], replicated, may hold values from -0.125 to 0.125
- routes: int32 [4096, 2], P('ep'), may hold values from 0 to 63, all different within a row; in each aligned block of 64 rows (0 to 63, 64 to 127, ...) at most 4 rows name the same one
- expert_gate_weight: bfloat16 [64, 2048, 1024], P('ep', None, 'tp'), may hold values from -0.125 to 0.125
- expert_up_weight: bfloat16 [64, 2048, 1024], P('ep', None, 'tp'), may hold values from -0.125 to 0.125
- expert_down_weight: bfloat16 [64, 1024, 2048], P('ep', 'tp'), may hold values from -0.1875 to 0.1875
- shared_gate_weight: bfloat16 [2048, 2048], P('tp', 'ep'), may hold values from -0.125 to 0.125
- shared_up_weight: bfloat16 [2048, 2048], P('tp', 'ep'), may hold values from -0.125 to 0.125
- shared_down_weight: bfloat16 [2048, 2048], P(None, 'tp'), may hold values from -0.125 to 0.125
Outputs:
- result: bfloat16 [4096, 2048], P('ep', 'tp')
- next_re: float32 [4096, 128, 64], P('ep', 'tp')
- next_im: float32 [4096, 128, 64], P('ep', 'tp')
Inputs may be any that keep to these rules, and one draw needn't show every extreme that they name: `routes`: each row names 2 different experts. Among the rows of one device no expert is named more than 4 times, and in every draw some expert is named exactly 4 times by some device's rows.
All inputs are finite; a program needn't handle non-finite values.
Results may differ from a plain program's by a relative error of at most 0.017.
Values may be sent and summed in bfloat16 or wider, within the bound.
A program may use at most 128 MiB of HBM per device.

v0:
```python
import jax
import jax.numpy as jnp
from jax import lax
from jax.sharding import PartitionSpec as P

NG = 4
EPS = 1e-06


def total_of_pieces(x, axis):
    blocks = lax.all_gather(x, axis)
    return blocks.sum(axis=0)


def in_blocks(x, dim, size):
    lengths = x.shape
    blocks = x.reshape(*lengths[:dim], size, lengths[dim] // size, *lengths[dim + 1 :])
    return jnp.moveaxis(blocks, dim, 0)


def sent_and_summed(x, axis, dim):
    blocks = in_blocks(x, dim, lax.axis_size(axis))
    arrived = lax.all_to_all(blocks, axis, split_axis=0, concat_axis=0, tiled=True)
    return arrived.astype(jnp.float32).sum(axis=0)


def sent_to_all(x, axis):
    size = lax.axis_size(axis)
    return lax.all_to_all(jnp.broadcast_to(x[None], (size, *x.shape)), axis, 0, 0, tiled=True)


def over_copies(x, axis):
    return sent_to_all(x, axis).sum(axis=0)


def in_one(arrays, axis):
    ends = [0]
    for a in arrays:
        ends.append(ends[-1] + a.size)
    so_far = over_copies(jnp.concatenate([a.ravel() for a in arrays]), axis)
    return tuple((so_far[b:e].reshape(a.shape) for a, b, e in zip(arrays, ends, ends[1:])))


def joined_along(blocks, dim):
    lengths = list(blocks.shape[1:])
    lengths[dim] *= blocks.shape[0]
    return jnp.moveaxis(blocks, 0, dim).reshape(lengths)


def collect(x, axis, dim):
    return joined_along(sent_to_all(x, axis), dim)


def taken_together(x, axis):
    return sent_to_all(x, axis).astype(jnp.float32).sum(axis=0)


def state_factors(rate, freq, log_group_step, input_map_real, input_map_imaginary):
    step_size = jnp.exp(log_group_step)[:, None]
    magnitude = jnp.exp(-rate * step_size)
    abar_re = magnitude * jnp.cos(freq * step_size)
    abar_im = magnitude * jnp.sin(freq * step_size)
    denom = rate * rate + freq * freq
    shift_re = abar_re - 1.0
    fac_re = (abar_im * freq - shift_re * rate) / denom
    fac_im = -(abar_im * rate + shift_re * freq) / denom
    bbar_re = fac_re[:, :, None] * input_map_real - fac_im[:, :, None] * input_map_imaginary
    bbar_im = fac_re[:, :, None] * input_map_imaginary + fac_im[:, :, None] * input_map_real
    return (abar_re, abar_im, bbar_re, bbar_im)


def state_step(
    normed,
    sequence_state_real,
    sequence_state_imaginary,
    factors,
    output_map_real,
    output_map_imaginary,
    skip,
):
    abar_re, abar_im, bbar_re, bbar_im = factors
    groups = abar_re.shape[0]
    inputs = normed.astype(jnp.float32)
    grouped = inputs.reshape(inputs.shape[0], groups, -1)
    drive_re = jnp.einsum("tgc,gpc->tgp", grouped, bbar_re)
    drive_im = jnp.einsum("tgc,gpc->tgp", grouped, bbar_im)
    fresh_real = abar_re * sequence_state_real - abar_im * sequence_state_imaginary + drive_re
    fresh_imaginary = abar_re * sequence_state_imaginary + abar_im * sequence_state_real + drive_im
    state_readout = jnp.einsum("dor,zdr->zdo", output_map_real, fresh_real)
    state_readout = state_readout - jnp.einsum(
        "dor,zdr->zdo", output_map_imaginary, fresh_imaginary
    )
    mixed = state_readout.reshape(inputs.shape) + skip * inputs
    return (mixed, fresh_real, fresh_imaginary)


def pair_product(left, first_map, second_map):
    first = jnp.dot(left, first_map, preferred_element_type=jnp.float32)
    second = jnp.dot(left, second_map, preferred_element_type=jnp.float32)
    return jnp.concatenate([first, second], axis=1)


def shards(
    tokens,
    sequence_state_real,
    sequence_state_imaginary,
    mixer_norm_gain,
    expert_norm_gain,
    rate,
    freq,
    log_group_step,
    input_map_real,
    input_map_imaginary,
    output_map_real,
    output_map_imaginary,
    skip,
    mixer_value_weight,
    mixer_gate_weight,
    group_router_weight,
    expert_router_weight,
    dense_blend_weight,
    routes,
    expert_gate_weight,
    expert_up_weight,
    expert_down_weight,
    shared_gate_weight,
    shared_up_weight,
    shared_down_weight,
):
    seq_rows, half_width = tokens.shape
    width = 2 * half_width
    column_start = lax.axis_index("tp") * half_width

    def own_rows(values):
        return lax.dynamic_slice_in_dim(values, column_start, half_width, 0)

    float_tokens = tokens.astype(jnp.float32)
    square_sum = total_of_pieces(jnp.sum(float_tokens * float_tokens, axis=1), "tp")
    first_scale = lax.rsqrt(square_sum / width + EPS)[:, None]
    normed = (float_tokens * first_scale * own_rows(mixer_norm_gain)).astype(jnp.bfloat16)
    factors = state_factors(rate, freq, log_group_step, input_map_real, input_map_imaginary)
    mixed, next_re, next_im = state_step(
        normed,
        sequence_state_real,
        sequence_state_imaginary,
        factors,
        output_map_real,
        output_map_imaginary,
        skip,
    )
    activated = jax.nn.gelu(mixed).astype(jnp.bfloat16)
    value_part = jnp.dot(activated, mixer_value_weight, preferred_element_type=jnp.float32)
    gate_part = jnp.dot(activated, mixer_gate_weight, preferred_element_type=jnp.float32)
    stacked = jnp.stack([value_part, gate_part], axis=1)
    mix_sum = sent_and_summed(stacked.astype(jnp.bfloat16), "tp", 2)
    mix_half = (mix_sum[:, 0] * jax.nn.sigmoid(mix_sum[:, 1])).astype(jnp.bfloat16)
    hidden = (float_tokens + mix_half.astype(jnp.float32)).astype(jnp.bfloat16)
    hidden_f32 = hidden.astype(jnp.float32)
    scaled = hidden_f32 * own_rows(expert_norm_gain)
    router_map = jnp.concatenate(
        [own_rows(group_router_weight), own_rows(expert_router_weight)], axis=1
    ).astype(jnp.float32)
    blend_map = own_rows(dense_blend_weight)
    hidden_squares = jnp.sum(hidden_f32 * hidden_f32, axis=1)
    total_squares = total_of_pieces(hidden_squares, "tp")
    inverse = lax.rsqrt(total_squares / width + EPS)[:, None]
    normal_rows = scaled * inverse
    raw_part = jnp.dot(normal_rows, router_map)
    blend_part = jnp.dot(normal_rows, blend_map)
    logits, blend_logit = in_one((raw_part, blend_part), "tp")
    hnorm = (scaled * inverse).astype(jnp.bfloat16)
    experts = expert_router_weight.shape[1]
    top_count = routes.shape[1]
    per_group = experts // NG
    group_prob = jax.nn.softmax(logits[:, :NG], axis=-1)
    expert_logits = logits[:, NG:]
    expert_hits = routes[:, :, None] == jnp.arange(experts, dtype=jnp.int32)[None, None, :]
    chosen = jnp.sum(jnp.where(expert_hits, expert_logits[:, None, :], 0.0), axis=2)
    group_hits = (routes // per_group)[:, :, None] == jnp.arange(NG, dtype=jnp.int32)[None, None, :]
    group_sel = jnp.sum(jnp.where(group_hits, group_prob[:, None, :], 0.0), axis=2)
    weights = jax.nn.softmax(chosen, axis=1) * group_sel
    full_rows = collect(hnorm, "tp", 1)
    capacity = max(2, 2 * seq_rows * top_count // experts)
    flat_routes = routes.reshape(-1)
    matches = (flat_routes[:, None] == jnp.arange(experts, dtype=jnp.int32)[None, :]).astype(
        jnp.int32
    )
    slot_rank = jnp.sum(jnp.cumsum(matches, axis=0) * matches, axis=1) - 1
    slot_target = flat_routes * capacity + slot_rank
    dispatch = slot_target[None, :] == jnp.arange(experts * capacity, dtype=jnp.int32)[:, None]
    dispatch_rows = jnp.sum(
        dispatch.reshape(experts * capacity, seq_rows, top_count).astype(jnp.float32), axis=2
    )
    outgoing = jnp.dot(
        dispatch_rows.astype(jnp.bfloat16), full_rows, preferred_element_type=jnp.float32
    )
    outgoing = outgoing.astype(jnp.bfloat16).reshape(experts, capacity, width)
    received = lax.all_to_all(outgoing, "ep", split_axis=0, concat_axis=0, tiled=True)
    sources = received.shape[0]
    items = received.shape[1]
    token_rows = received.reshape(sources * items, width)
    gate_e = jnp.dot(token_rows, expert_gate_weight[0], preferred_element_type=jnp.float32)
    expert_up_rows = jnp.dot(token_rows, expert_up_weight[0], preferred_element_type=jnp.float32)
    inner = (jax.nn.silu(gate_e) * expert_up_rows).astype(jnp.bfloat16)
    part_out = jnp.dot(inner, expert_down_weight[0], preferred_element_type=jnp.float32)
    total = taken_together(part_out.astype(jnp.bfloat16), "tp").astype(jnp.float32)
    total = lax.dynamic_slice_in_dim(total, column_start, half_width, 1)
    finished = total.astype(jnp.bfloat16).reshape(sources, items, half_width)
    returned = lax.all_to_all(finished, "ep", split_axis=0, concat_axis=0, tiled=True)
    returned_flat = returned.reshape(experts * capacity, half_width)
    picked = returned_flat[slot_target].reshape(seq_rows, top_count, half_width).astype(jnp.float32)
    routed = jnp.sum(weights[:, :, None] * picked, axis=1)
    partial_dense = pair_product(
        lax.all_gather(hnorm, "ep", axis=0, tiled=True), shared_gate_weight, shared_up_weight
    )
    dense_sum = taken_together(partial_dense.astype(jnp.bfloat16), "tp").astype(jnp.float32)
    dense_cols = shared_gate_weight.shape[1]
    inner_cols = (jax.nn.silu(dense_sum[:, :dense_cols]) * dense_sum[:, dense_cols:]).astype(
        jnp.bfloat16
    )
    dense_inner = lax.all_to_all(inner_cols, "ep", split_axis=0, concat_axis=1, tiled=True)
    dense_out = jnp.dot(dense_inner, shared_down_weight, preferred_element_type=jnp.float32)
    result = hidden_f32 + routed + jax.nn.sigmoid(blend_logit)[:, None] * dense_out
    return (result.astype(jnp.bfloat16), next_re, next_im)


def solution(mesh):
    placed = (
        P("ep", "tp"),
        P("ep", "tp", None),
        P("ep", "tp", None),
        P(),
        P(),
        P("tp", None),
        P("tp", None),
        P("tp"),
        P("tp", None, None),
        P("tp", None, None),
        P("tp", None, None),
        P("tp", None, None),
        P("tp"),
        P("tp", None),
        P("tp", None),
        P(),
        P(),
        P(),
        P("ep", None),
        P("ep", None, "tp"),
        P("ep", None, "tp"),
        P("ep", "tp", None),
        P("tp", "ep"),
        P("tp", "ep"),
        P(None, "tp"),
    )
    return jax.shard_map(
        shards,
        mesh=mesh,
        in_specs=placed,
        out_specs=(P("ep", "tp"), P("ep", "tp", None), P("ep", "tp", None)),
        check_vma=False,
    )
```

profile of v0, /device:TPU:0, one launch (start us, length us, event | category | flops | bytes accessed | tf_op | source)
XLA Modules:
  0.0 192.3 jit_solution(11711179658692557491)
XLA Ops:
  7.2 3.5 %copy.204 = f32[64,64,64]{0,2,1:T(8,128)} copy(f32[64,64,64]{2,1,0:T(8,128)} %param.27) | data formatting | bytes 2097152 | tf_op args[2]
  10.7 3.4 %copy.203 = f32[64,64,64]{0,2,1:T(8,128)} copy(f32[64,64,64]{2,1,0:T(8,128)} %param.26) | data formatting | bytes 2097152 | tf_op args[1]
  14.3 0.6 dynamic-slice
  15.5 0.2 dynamic-update-slice
  15.8 2.4 %all-reduce = f32[128]{0:T(128)S(1)} all-reduce(f32[128]{0:T(128)S(1)} %dynamic-update-slice), channel_id=2, replica_groups=mesh['ep'=64,'tp'=2] {'tp'}, use_global_device_ids=true, to_apply=%add | all-reduce | flops 128 | bytes 1024
  18.4 0.8 fusion.29
  19.1 1.1 copy.205
  20.2 1.0 fusion.65
  21.3 4.0 %bitcast_add_fusion.1 = f32[64,64,64]{0,2,1:T(8,128)S(1)} fusion(f32[64,64,64]{0,2,1:T(8,128)} %copy.204, f32[64,64,64]{0,2,1:T(8,128)} %copy.203, bf16[64,64,16]{0,2,1:T(8,128)(2,1)S(1)} %bitcast.73, f32[64,64]{1,0:T(8,128)S(1)} %get-tuple-element.30, f32[64,64]{1,0:T(8,128)S(1)} %get-tuple-element.31, f32[64,64,16]{1,2,0:T(8,128)S(1)} %copy-done.8, ...), kind=kOutput, calls=%fused_computation.14 | convolution fusion | flops 9633792 | bytes 3866624 | tf_op jit(solution)/shard_map/tgc,gpc->tgp/dot_general | solution.py:85
  25.3 2.4 %bitcast_add_fusion = f32[64,64,64]{0,2,1:T(8,128)S(1)} fusion(f32[64,64,64]{0,2,1:T(8,128)S(1)} %copy-done.6, f32[64,64,64]{0,2,1:T(8,128)S(1)} %copy-done.5, bf16[64,64,16]{0,2,1:T(8,128)(2,1)S(1)} %bitcast.74, f32[64,64]{1,0:T(8,128)S(1)} %get-tuple-element.30, f32[64,64]{1,0:T(8,128)S(1)} %get-tuple-element.31, f32[64,64,16]{1,2,0:T(8,128)S(1)} %copy-done.9, ...), kind=kOutput, calls=%fused_computation.13 | convolution fusion | flops 9633792 | bytes 3866624 | tf_op jit(solution)/shard_map/tgc,gpc->tgp/dot_general | solution.py:86
  27.8 0.4 fusion.78
  28.2 1.0 copy-done.10
  29.2 0.4 convolution_subtract_fusion
  29.6 0.2 copy.210
  29.9 3.1 %convolution_convert_fusion.4 = bf16[64,2048]{1,0:T(8,128)(2,1)S(1)} fusion(bf16[1024,2048]{1,0:T(8,128)(2,1)} %param.39, f32[64,1024]{1,0:T(8,128)S(1)} %copy.210, f32[1024]{0:T(1024)S(1)} %copy-done.17, f32[1024]{0:T(1024)S(1)} %dynamic_slice.18, f32[64]{0:T(128)S(1)} %add_rsqrt_fusion.1, bf16[64,1024]{1,0:T(8,128)(2,1)S(1)} %copy-done.7), kind=kOutput, calls=%fused_computation.6 | convolution fusion | flops 269615104 | bytes 4858112 | tf_op jit(solution)/shard_map/dot_general | solution.py:153
  33.0 0.2 stack.10
  33.3 3.1 %convolution_convert_fusion.5 = bf16[64,2048]{1,0:T(8,128)(2,1)S(1)} fusion(bf16[1024,2048]{1,0:T(8,128)(2,1)} %param.38, f32[64,1024]{1,0:T(8,128)S(1)} %copy.210, f32[1024]{0:T(1024)S(1)} %copy-done.17, f32[1024]{0:T(1024)S(1)} %dynamic_slice.18, f32[64]{0:T(128)S(1)} %add_rsqrt_fusion.1, bf16[64,1024]{1,0:T(8,128)(2,1)S(1)} %copy-done.7), kind=kOutput, calls=%fused_computation.7 | convolution fusion | flops 269615104 | bytes 4858112 | tf_op jit(solution)/shard_map/dot_general | solution.py:152
  36.4 0.2 stack.9
  36.8 4.3 %all_to_all.57 = bf16[2,64,2,1024]{3,1,2,0:T(8,128)(2,1)S(1)} all-to-all(bf16[2,64,2,1024]{3,1,2,0:T(8,128)(2,1)S(1)} %maximum_bitcast_fusion), channel_id=1, replica_groups=mesh['ep'=64,'tp'=2] {'tp'}, dimensions={0} | all-to-all | bytes 1048576 | tf_op jit(solution)/shard_map/all_to_all | solution.py:23
  41.2 0.2 fusion.44
  41.4 0.2 dynamic-update-slice.1
  41.6 2.4 %all-reduce.1 = f32[128]{0:T(128)S(1)} all-reduce(f32[128]{0:T(128)S(1)} %dynamic-update-slice.1), channel_id=3, replica_groups=mesh['ep'=64,'tp'=2] {'tp'}, use_global_device_ids=true, to_apply=%add.1 | all-reduce | flops 128 | bytes 1024
  44.2 0.7 fusion.40
  45.0 1.6 broadcast_in_dim.33
  46.6 3.4 %all-to-all-start.2 = ((bf16[2,64,1024]{2,1,0:T(8,128)(2,1)}), bf16[2,64,1024]{2,1,0:T(8,128)(2,1)S(1)}, u32[]{:S(2)}, u32[]{:S(2)}) async-start(bf16[2,64,1024]{2,1,0:T(8,128)(2,1)} %broadcast_in_dim.33), calls=%async_computation.2 | async-start | bytes 524288 | tf_op jit(solution)/shard_map/all_to_all | solution.py:29
  50.1 0.2 fusion.42
  50.5 0.2 convolution_bitcast_fusion
  50.7 0.9 all-to-all-done.2
  51.6 0.6 broadcast_in_dim.24
  52.2 3.9 %all-to-all-start.1 = ((f32[2,1,4416]{2,1,0:T(1,128)}), f32[2,1,4416]{2,1,0:T(1,128)}, u32[]{:S(2)}, u32[]{:S(2)}) async-start(f32[2,1,4416]{2,1,0:T(1,128)} %broadcast_in_dim.24), calls=%async_computation.1 | async-start | bytes 71680 | tf_op jit(solution)/shard_map/all_to_all | solution.py:29
  56.6 0.2 reduce_window_sum.11
  56.8 0.2 select_reduce_fusion
  57.1 0.7 add_select_fusion
  57.9 0.4 convolution_convert_fusion.3
  58.4 1.2 reshape.198
  59.6 11.7 %all-to-all-start.3 = ((bf16[64,4,2048]{2,1,0:T(4,128)(2,1)}), bf16[64,4,2048]{2,1,0:T(4,128)(2,1)S(1)}, u32[]{:S(2)}, u32[]{:S(2)}) async-start(bf16[64,4,2048]{2,1,0:T(4,128)(2,1)} %reshape.198), calls=%async_computation.3 | async-start | bytes 2097152 | tf_op jit(solution)/shard_map/all_to_all | solution.py:198
  71.3 0.8 reduce_sum.140
  72.5 0.2 select_reduce_fusion.1
  72.8 3.8 %copy.229 = f32[64,64,64]{2,1,0:T(8,128)} copy(f32[64,64,64]{0,2,1:T(8,128)} %copy-done.4) | data formatting | bytes 2097152
  76.5 3.8 %copy.230 = f32[64,64,64]{2,1,0:T(8,128)} copy(f32[64,64,64]{0,2,1:T(8,128)} %copy-done.3) | data formatting | bytes 2097152
  80.7 12.7 %all-to-all-done.3 = bf16[64,4,2048]{2,1,0:T(4,128)(2,1)S(1)} async-done(((bf16[64,4,2048]{2,1,0:T(4,128)(2,1)}), bf16[64,4,2048]{2,1,0:T(4,128)(2,1)S(1)}, u32[]{:S(2)}, u32[]{:S(2)}) %all-to-all-start.3) | async-done | bytes 1048608 | tf_op jit(solution)/shard_map/all_to_all | solution.py:198
  93.4 1.2 reshape.199
  94.6 3.4 %fusion.3 = f32[256,512]{1,0:T(8,128)} fusion(bf16[256,2048]{1,0:T(8,128)(2,1)} %reshape.199, bf16[1,2048,512]{2,1,0:T(8,128)(2,1)} %param.44), kind=kOutput, calls=%fused_computation.11 | convolution fusion | flops 536870912 | bytes 3670016 | tf_op jit(solution)/shard_map/dot_general | solution.py:202
  98.0 3.3 %convolution_convert_fusion.2 = bf16[256,2048]{1,0:T(8,128)(2,1)S(1)} fusion(bf16[1,512,2048]{2,1,0:T(8,128)(2,1)S(1)} %copy-done, bf16[256,2048]{1,0:T(8,128)(2,1)} %reshape.199, bf16[1,2048,512]{2,1,0:T(8,128)(2,1)} %param.45, f32[256,512]{1,0:T(8,128)} %fusion.3), kind=kOutput, calls=%fused_computation.4 | convolution fusion | flops 1075052544 | bytes 6815744 | tf_op jit(solution)/shard_map/dot_general | solution.py:205
  101.3 0.2 broadcast_in_dim.34
  101.6 5.4 %all_to_all.55 = bf16[2,256,2048]{2,1,0:T(8,128)(2,1)S(1)} all-to-all(bf16[2,256,2048]{2,1,0:T(8,128)(2,1)S(1)} %broadcast_in_dim.34), channel_id=1, replica_groups=mesh['ep'=64,'tp'=2] {'tp'}, dimensions={0} | all-to-all | bytes 4194304 | tf_op jit(solution)/shard_map/all_to_all | solution.py:29
  107.0 0.4 convert_reduce_fusion
  107.5 1.0 reshape.200
  108.5 21.7 %all-gather.4.cloned.1.call-done = bf16[4096,1024]{1,0:T(8,128)(2,1)} async-done(((bf16[64,1024]{1,0:T(8,128)(2,1)}), bf16[4096,1024]{1,0:T(8,128)(2,1)}) %all-gather.4.cloned.1.call-update) | async-done | bytes 8388624 | tf_op jit(solution)/shard_map/all_gather | solution.py:214
  130.2 6.1 %convolution_convert_fusion = bf16[4096,32]{0,1:T(8,128)(2,1)S(1)} fusion(bf16[4096,1024]{1,0:T(8,128)(2,1)} %all-gather.4.cloned.1.call-done, bf16[1024,32]{0,1:T(8,128)(2,1)S(1)} %copy-done.14), kind=kOutput, calls=%fused_computation.1 | convolution fusion | flops 268566528 | bytes 8716288 | tf_op jit(solution)/shard_map/dot_general | solution.py:99
  136.3 2.5 %convolution_convert_fusion.1 = bf16[4096,32]{0,1:T(8,128)(2,1)S(1)} fusion(bf16[4096,1024]{1,0:T(8,128)(2,1)S(1)} %copy-done.2, bf16[1024,32]{0,1:T(8,128)(2,1)S(1)} %copy-done.15), kind=kOutput, calls=%fused_computation.2 | convolution fusion | flops 268566528 | bytes 8716288 | tf_op jit(solution)/shard_map/dot_general | solution.py:98
  139.0 4.6 %all_to_all.56 = bf16[2,4096,64]{1,2,0:T(8,128)(2,1)S(1)} all-to-all(bf16[2,4096,64]{1,2,0:T(8,128)(2,1)S(1)} %broadcast_in_dim.35), channel_id=1, replica_groups=mesh['ep'=64,'tp'=2] {'tp'}, dimensions={0} | all-to-all | bytes 2097152 | tf_op jit(solution)/shard_map/all_to_all | solution.py:29
  143.6 8.6 %all-to-all-start.5 = ((bf16[64,4,1024]{2,1,0:T(4,128)(2,1)}), bf16[64,4,1024]{2,1,0:T(4,128)(2,1)S(1)}, u32[]{:S(2)}, u32[]{:S(2)}) async-start(bf16[64,4,1024]{2,1,0:T(4,128)(2,1)} %reshape.200), calls=%async_computation.5 | async-start | bytes 1048576 | tf_op jit(solution)/shard_map/all_to_all | solution.py:209
  152.5 0.5 all_to_all.43
  153.1 0.3 copy.246
  153.4 1.0 reshape.228
  154.4 11.4 %all-to-all-done.5 = bf16[64,4,1024]{2,1,0:T(4,128)(2,1)S(1)} async-done(((bf16[64,4,1024]{2,1,0:T(4,128)(2,1)}), bf16[64,4,1024]{2,1,0:T(4,128)(2,1)S(1)}, u32[]{:S(2)}, u32[]{:S(2)}) %all-to-all-start.5) | async-done | bytes 524320 | tf_op jit(solution)/shard_map/all_to_all | solution.py:209
  165.9 5.0 %all-to-all-start.7 = ((bf16[64,2,1024]{2,1,0:T(2,128)(2,1)}), bf16[64,2,1024]{2,1,0:T(2,128)(2,1)S(1)}, u32[]{:S(2)}, u32[]{:S(2)}) async-start(bf16[64,2,1024]{2,1,0:T(2,128)(2,1)} %reshape.228), calls=%async_computation.7 | async-start | bytes 524288 | tf_op jit(solution)/shard_map/all_to_all | solution.py:221
  171.0 0.9 gather_fusion
  171.8 0.3 reshape.203
  172.2 0.7 multiply_reduce_fusion
  172.9 8.3 %all-to-all-done.7 = bf16[64,2,1024]{2,1,0:T(2,128)(2,1)S(1)} async-done(((bf16[64,2,1024]{2,1,0:T(2,128)(2,1)}), bf16[64,2,1024]{2,1,0:T(2,128)(2,1)S(1)}, u32[]{:S(2)}, u32[]{:S(2)}) %all-to-all-start.7) | async-done | bytes 262176 | tf_op jit(solution)/shard_map/all_to_all | solution.py:221
  181.2 0.3 reshape.229
  181.6 3.9 %fusion.12 = bf16[64,1024]{1,0:T(8,128)(2,1)} fusion(bf16[64,2048]{0,1:T(8,128)(2,1)S(1)} %bitcast.77, bf16[2048,1024]{1,0:T(8,128)(2,1)} %param.49, f32[64,1024]{1,0:T(8,128)S(1)} %multiply_reduce_fusion, bf16[64,1024]{1,0:T(8,128)(2,1)S(1)} %get-tuple-element.28, f32[64]{0:T(128)S(1)} %fusion.73), kind=kOutput, calls=%fused_computation.21 | convolution fusion | flops 268763136 | bytes 4980992 | tf_op jit(solution)/shard_map/dot_general | solution.py:222
  (104 shorter events, 3.2 us)
Async XLA Ops:
  7.2 90.8 %copy-start = (bf16[1,512,2048]{2,1,0:T(8,128)(2,1)S(1)}, bf16[1,512,2048]{2,1,0:T(8,128)(2,1)}, u32[]{:S(2)}) copy-start(bf16[1,512,2048]{2,1,0:T(8,128)(2,1)} %param.46) | copy-start | bytes 6291460
  7.2 123.0 %all-gather.4.cloned.1.call-start = ((), (), s32[]{:S(2)}) async-start(), calls=%async_computation.8 | async-start | bytes 8519680 | tf_op jit(solution)/shard_map/all_gather | solution.py:214
  10.7 3.5 %copy-start.7 = (bf16[64,1024]{1,0:T(8,128)(2,1)S(1)}, bf16[64,1024]{1,0:T(8,128)(2,1)}, u32[]{:S(2)}) copy-start(bf16[64,1024]{1,0:T(8,128)(2,1)} %param.25) | copy-start | bytes 393220
  10.7 3.6 %copy-start.23 = (u32[128]{0:T(128)S(1)}, u32[128]{0:T(128)}, u32[]{:S(2)}) copy-start(u32[128]{0:T(128)} %constant.69) | copy-start | bytes 1540
  10.7 7.6 %copy-start.20 = (f32[2048]{0:T(1024)S(1)}, f32[2048]{0:T(1024)}, u32[]{:S(2)}) copy-start(f32[2048]{0:T(1024)} %param.28) | copy-start | bytes 24580
  10.7 9.5 %copy-start.22 = (f32[64]{0:T(128)S(1)}, f32[64]{0:T(128)}, u32[]{:S(2)}) copy-start(f32[64]{0:T(128)} %param.32) | copy-start | bytes 772
  10.7 10.5 %copy-start.8 = (f32[64,64,16]{1,2,0:T(8,128)S(1)}, f32[64,64,16]{1,2,0:T(8,128)}, u32[]{:S(2)}) copy-start(f32[64,64,16]{1,2,0:T(8,128)} %param.34) | copy-start | bytes 786436
  10.7 10.5 %copy-start.9 = (f32[64,64,16]{1,2,0:T(8,128)S(1)}, f32[64,64,16]{1,2,0:T(8,128)}, u32[]{:S(2)}) copy-start(f32[64,64,16]{1,2,0:T(8,128)} %param.33) | copy-start | bytes 786436
  21.2 4.0 %copy-start.5 = (f32[64,64,64]{0,2,1:T(8,128)S(1)}, f32[64,64,64]{0,2,1:T(8,128)}, u32[]{:S(2)}) copy-start(f32[64,64,64]{0,2,1:T(8,128)} %copy.204) | copy-start | bytes 3145732
  21.2 4.0 %copy-start.6 = (f32[64,64,64]{0,2,1:T(8,128)S(1)}, f32[64,64,64]{0,2,1:T(8,128)}, u32[]{:S(2)}) copy-start(f32[64,64,64]{0,2,1:T(8,128)} %copy.203) | copy-start | bytes 3145732
  25.3 2.5 %copy-start.4 = (f32[64,64,64]{0,2,1:T(8,128)}, f32[64,64,64]{0,2,1:T(8,128)S(1)}, u32[]{:S(2)}) copy-start(f32[64,64,64]{0,2,1:T(8,128)S(1)} %bitcast_add_fusion.1) | copy-start | bytes 3145732
  25.3 2.5 %copy-start.11 = (f32[64,16,64]{2,1,0:T(8,128)S(1)}, f32[64,16,64]{2,1,0:T(8,128)}, u32[]{:S(2)}) copy-start(f32[64,16,64]{2,1,0:T(8,128)} %param.35) | copy-start | bytes 786436
  27.8 1.9 copy-start.3
  27.8 1.4 copy-start.10
  29.2 0.7 copy-start.17
  36.7 7.5 %copy-start.21 = (f32[2048]{0:T(1024)S(1)}, f32[2048]{0:T(1024)}, u32[]{:S(2)}) copy-start(f32[2048]{0:T(1024)} %param.29) | copy-start | bytes 24580
  36.8 13.3 %copy-start.19 = (bf16[2048,4]{0,1:T(4,128)(2,1)S(1)}, bf16[2048,4]{0,1:T(4,128)(2,1)}, u32[]{:S(2)}) copy-start(bf16[2048,4]{0,1:T(4,128)(2,1)} %param.40) | copy-start | bytes 49156
  36.8 13.3 %copy-start.16 = (bf16[2048,64]{0,1:T(8,128)(2,1)S(1)}, bf16[2048,64]{0,1:T(8,128)(2,1)}, u32[]{:S(2)}) copy-start(bf16[2048,64]{0,1:T(8,128)(2,1)} %param.41) | copy-start | bytes 786436
  41.1 9.4 %dynamic-slice-start = ((f32[2048]{0:T(1024)}, s32[]{:T(128)}), f32[1024]{0:T(1024)S(1)}, s32[]{:S(2)}) async-start(f32[2048]{0:T(1024)} %param.42, s32[]{:T(128)} %select_n.31), calls=%async_computation.9 | async-start | bytes 8704 | tf_op jit(solution)/shard_map/dynamic_slice | solution.py:135
  41.2 15.0 %copy-start.18 = (s32[64,2]{0,1:T(2,128)S(1)}, s32[64,2]{0,1:T(2,128)}, u32[]{:S(2)}) copy-start(s32[64,2]{0,1:T(2,128)} %param.43) | copy-start | bytes 1540
  46.6 5.0 %all-to-all-start.2 = ((bf16[2,64,1024]{2,1,0:T(8,128)(2,1)}), bf16[2,64,1024]{2,1,0:T(8,128)(2,1)S(1)}, u32[]{:S(2)}, u32[]{:S(2)}) async-start(bf16[2,64,1024]{2,1,0:T(8,128)(2,1)} %broadcast_in_dim.33), calls=%async_computation.2 | async-start | bytes 524288 | tf_op jit(solution)/shard_map/all_to_all | solution.py:29
  52.2 7.4 %all-to-all-start.1 = ((f32[2,1,4416]{2,1,0:T(1,128)}), f32[2,1,4416]{2,1,0:T(1,128)}, u32[]{:S(2)}, u32[]{:S(2)}) async-start(f32[2,1,4416]{2,1,0:T(1,128)} %broadcast_in_dim.24), calls=%async_computation.1 | async-start | bytes 71680 | tf_op jit(solution)/shard_map/all_to_all | solution.py:29
  59.6 33.8 %all-to-all-start.3 = ((bf16[64,4,2048]{2,1,0:T(4,128)(2,1)}), bf16[64,4,2048]{2,1,0:T(4,128)(2,1)S(1)}, u32[]{:S(2)}, u32[]{:S(2)}) async-start(bf16[64,4,2048]{2,1,0:T(4,128)(2,1)} %reshape.198), calls=%async_computation.3 | async-start | bytes 2097152 | tf_op jit(solution)/shard_map/all_to_all | solution.py:198
  76.5 3.8 %copy-start.13 = (s32[64,2]{1,0:T(8,128)S(1)}, s32[64,2]{1,0:T(8,128)}, u32[]{:S(2)}) copy-start(s32[64,2]{1,0:T(8,128)} %get-tuple-element.35) | copy-start | bytes 1540
  76.5 3.9 %copy-start.12 = (s32[64,2]{1,0:T(8,128)S(1)}, s32[64,2]{1,0:T(8,128)}, u32[]{:S(2)}) copy-start(s32[64,2]{1,0:T(8,128)} %get-tuple-element.33) | copy-start | bytes 1540
  107.0 23.2 %copy-start.14 = (bf16[1024,32]{0,1:T(8,128)(2,1)S(1)}, bf16[1024,32]{0,1:T(8,128)(2,1)}, u32[]{:S(2)}) copy-start(bf16[1024,32]{0,1:T(8,128)(2,1)} %param.48) | copy-start | bytes 196612
  108.5 27.8 %copy-start.15 = (bf16[1024,32]{0,1:T(8,128)(2,1)S(1)}, bf16[1024,32]{0,1:T(8,128)(2,1)}, u32[]{:S(2)}) copy-start(bf16[1024,32]{0,1:T(8,128)(2,1)} %param.47) | copy-start | bytes 196612
  130.2 6.1 %copy-start.2 = (bf16[4096,1024]{1,0:T(8,128)(2,1)S(1)}, bf16[4096,1024]{1,0:T(8,128)(2,1)}, u32[]{:S(2)}) copy-start(bf16[4096,1024]{1,0:T(8,128)(2,1)} %all-gather.4.cloned.1.call-done) | copy-start | bytes 25165828
  143.6 22.3 %all-to-all-start.5 = ((bf16[64,4,1024]{2,1,0:T(4,128)(2,1)}), bf16[64,4,1024]{2,1,0:T(4,128)(2,1)S(1)}, u32[]{:S(2)}, u32[]{:S(2)}) async-start(bf16[64,4,1024]{2,1,0:T(4,128)(2,1)} %reshape.200), calls=%async_computation.5 | async-start | bytes 1048576 | tf_op jit(solution)/shard_map/all_to_all | solution.py:209
  165.9 15.3 %all-to-all-start.7 = ((bf16[64,2,1024]{2,1,0:T(2,128)(2,1)}), bf16[64,2,1024]{2,1,0:T(2,128)(2,1)S(1)}, u32[]{:S(2)}, u32[]{:S(2)}) async-start(bf16[64,2,1024]{2,1,0:T(2,128)(2,1)} %reshape.228), calls=%async_computation.7 | async-start | bytes 524288 | tf_op jit(solution)/shard_map/all_to_all | solution.py:221
  181.6 3.9 %copy-start.1 = (bf16[1,512,2048]{2,1,0:T(8,128)(2,1)S(1)}, bf16[1,512,2048]{2,1,0:T(8,128)(2,1)}, u32[]{:S(2)}) copy-start(bf16[1,512,2048]{2,1,0:T(8,128)(2,1)} %param.46) | copy-start | bytes 6291460
Sparse Core Ops, SparseCore 0:
  45.1 85.0 all-gather.3
where the time goes:
time: 193 us; the launch traced here: 192 us
  waiting for transfers between devices  55 us (28%)
  matrix products  33.7 us (17%)
  starting transfers between devices  32.6 us (17%)
  local copies, waits for them, and re-layouts  29.5 us (15%)
  blocking collectives  19.2 us (10%)
  between operations  15.3 us (8%)
  other arithmetic  6.95 us (4%)
    all_gather x1, waiting for transfers between devices, shards(): lax.all_gather(hnorm, 'ep', axis=0, tiled=True)  21.7 us
    unnamed x61, local copies, waits for them, and re-layouts  18.2 us
    all_to_all x1, waiting for transfers between devices, shards(): lax.all_to_all(outgoing, 'ep', split_axis=0, concat_axis=0, tiled=True)  12.7 us
    all_to_all x1, starting transfers between devices, shards(): lax.all_to_all(outgoing, 'ep', split_axis=0, concat_axis=0, tiled=True)  11.7 us
    all_to_all x1, waiting for transfers between devices, shards(): lax.all_to_all(finished, 'ep', split_axis=0, concat_axis=0, tiled=True)  11.4 us
    all_to_all x2, blocking collectives, sent_to_all(): lax.all_to_all(jnp.broadcast_to(x[None], (size, *x.shape)), axis, 0, 0, t...  9.99 us
    all_to_all x1, starting transfers between devices, shards(): lax.all_to_all(finished, 'ep', split_axis=0, concat_axis=0, tiled=True)  8.6 us
    all_to_all x1, waiting for transfers between devices, shards(): lax.all_to_all(inner_cols, 'ep', split_axis=0, concat_axis=1, tiled=True)  8.32 us
  transfers between devices with their start and end apart: 6, of which 5 were waited for; matrix products, arithmetic and copies ran while one was open for 15% of the time, Pallas kernels for 0%

commit v1 on v0

--- a/solution.py
+++ b/solution.py
@@ -211,7 +211,11 @@
     picked = returned_flat[slot_target].reshape(seq_rows, top_count, half_width).astype(jnp.float32)
     routed = jnp.sum(weights[:, :, None] * picked, axis=1)
     partial_dense = pair_product(
-        lax.all_gather(hnorm, "ep", axis=0, tiled=True), shared_gate_weight, shared_up_weight
+        jnp.concatenate(
+            lax.all_to_all(jnp.stack([hnorm] * lax.axis_size("ep")), "ep", 0, 0), axis=0
+        ),
+        shared_gate_weight,
+        shared_up_weight,
     )
     dense_sum = taken_together(partial_dense.astype(jnp.bfloat16), "tp").astype(jnp.float32)
     dense_cols = shared_gate_weight.shape[1]

time: 193 us -> 293 us (1.52)
  waiting for transfers between devices: 55 us -> 146 us
  starting transfers between devices: 32.6 us -> 46.1 us
  between operations: 15.3 us -> 1.97 us
  matrix products: 33.7 us -> 37.9 us
  local copies, waits for them, and re-layouts: 29.5 us -> 33.4 us
    all_to_all x0 -> x1, waiting for transfers between devices: none -> 107 us  [shards(): lax.all_to_all(jnp.stack([hnorm] * lax.axis_size('ep')), 'ep', 0, 0)]
    all_gather x1 -> x0, waiting for transfers between devices: 21.7 us -> none  [shards(): lax.all_gather(hnorm, 'ep', axis=0, tiled=True)]
    all_to_all x1, starting transfers between devices: 8.6 us -> 16.9 us  [shards(): lax.all_to_all(finished, 'ep', split_axis=0, concat_axis=0, tiled=True)]
    all_to_all x0 -> x1, starting transfers between devices: none -> 5.93 us  [shards(): lax.all_to_all(jnp.stack([hnorm] * lax.axis_size('ep')), 'ep', 0, 0)]
    all_to_all x1, waiting for transfers between devices: 12.7 us -> 17.7 us  [shards(): lax.all_to_all(outgoing, 'ep', split_axis=0, concat_axis=0, tiled=True)]
    another operation x0 -> x1, local copies, waits for them, and re-layouts: none -> 4.28 us  [shards(): jnp.stack([hnorm] * lax.axis_size('ep'))]
    dot_general x1, matrix products: 2.55 us -> 5.93 us  [pair_product(): first = jnp.dot(left, first_map, preferred_element_type=jnp.float32)]
    unnamed x61 -> x55, local copies, waits for them, and re-layouts: 18.2 us -> 17.3 us
  transfers between devices with their start and end apart: 6 -> 6, of which waited for: 5 -> 5; matrix products, arithmetic and copies ran while one was open for 15% -> 8% of each run, Pallas kernels for 0% -> 0%
where the time goes in v1:
time: 293 us; the launch traced here: 292 us
  waiting for transfers between devices  146 us (50%)
  starting transfers between devices  46.1 us (16%)
  matrix products  37.9 us (13%)
  local copies, waits for them, and re-layouts  33.4 us (11%)
  blocking collectives  19.9 us (7%)
  other arithmetic  6.54 us (2%)
    all_to_all x1, waiting for transfers between devices, shards(): lax.all_to_all(jnp.stack([hnorm] * lax.axis_size('ep')), 'ep', 0, 0)  107 us
    all_to_all x1, waiting for transfers between devices, shards(): lax.all_to_all(outgoing, 'ep', split_axis=0, concat_axis=0, tiled=True)  17.7 us
    unnamed x55, local copies, waits for them, and re-layouts  17.3 us
    all_to_all x1, starting transfers between devices, shards(): lax.all_to_all(finished, 'ep', split_axis=0, concat_axis=0, tiled=True)  16.9 us
    all_to_all x1, starting transfers between devices, shards(): lax.all_to_all(outgoing, 'ep', split_axis=0, concat_axis=0, tiled=True)  11.5 us
    all_to_all x1, waiting for transfers between devices, shards(): lax.all_to_all(finished, 'ep', split_axis=0, concat_axis=0, tiled=True)  11.4 us
    all_to_all x2, blocking collectives, sent_to_all(): lax.all_to_all(jnp.broadcast_to(x[None], (size, *x.shape)), axis, 0, 0, t...  10.9 us
    all_to_all x1, waiting for transfers between devices, shards(): lax.all_to_all(inner_cols, 'ep', split_axis=0, concat_axis=1, tiled=True)  8.32 us
  transfers between devices with their start and end apart: 6, of which 5 were waited for; matrix products, arithmetic and copies ran while one was open for 8% of the time, Pallas kernels for 0%

profile of v1, /device:TPU:0, one launch (start us, length us, event | category | flops | bytes accessed | tf_op | source)
XLA Modules:
  0.0 291.9 jit_solution(5431180281741382593)
XLA Ops:
  0.7 3.5 %copy.204 = f32[64,64,64]{0,2,1:T(8,128)} copy(f32[64,64,64]{2,1,0:T(8,128)} %param.27) | data formatting | bytes 2097152 | tf_op args[2]
  4.2 3.4 %copy.203 = f32[64,64,64]{0,2,1:T(8,128)} copy(f32[64,64,64]{2,1,0:T(8,128)} %param.26) | data formatting | bytes 2097152 | tf_op args[1]
  7.7 0.6 dynamic-slice
  9.0 0.2 dynamic-update-slice
  9.2 2.4 all-reduce
  11.8 0.8 fusion.29
  12.5 1.1 copy.205
  13.6 1.0 fusion.65
  14.7 4.0 %bitcast_add_fusion.1 = f32[64,64,64]{0,2,1:T(8,128)S(1)} fusion(f32[64,64,64]{0,2,1:T(8,128)} %copy.204, f32[64,64,64]{0,2,1:T(8,128)} %copy.203, bf16[64,64,16]{0,2,1:T(8,128)(2,1)S(1)} %bitcast.74, f32[64,64]{1,0:T(8,128)S(1)} %get-tuple-element.30, f32[64,64]{1,0:T(8,128)S(1)} %get-tuple-element.31, f32[64,64,16]{1,2,0:T(8,128)S(1)} %copy-done.8, ...), kind=kOutput, calls=%fused_computation.14 | convolution fusion | flops 9633792 | bytes 3866624 | tf_op jit(solution)/shard_map/tgc,gpc->tgp/dot_general | solution.py:85
  18.7 2.4 bitcast_add_fusion
  21.2 0.4 fusion.78
  21.6 1.0 copy-done.10
  22.6 0.4 convolution_subtract_fusion
  23.1 0.2 copy.210
  23.3 3.1 %convolution_convert_fusion.4 = bf16[64,2048]{1,0:T(8,128)(2,1)S(1)} fusion(bf16[1024,2048]{1,0:T(8,128)(2,1)} %param.39, f32[64,1024]{1,0:T(8,128)S(1)} %copy.210, f32[1024]{0:T(1024)S(1)} %copy-done.14, f32[1024]{0:T(1024)S(1)} %dynamic_slice.18, f32[64]{0:T(128)S(1)} %add_rsqrt_fusion.1, bf16[64,1024]{1,0:T(8,128)(2,1)S(1)} %copy-done.7), kind=kOutput, calls=%fused_computation.6 | convolution fusion | flops 269615104 | bytes 4858112 | tf_op jit(solution)/shard_map/dot_general | solution.py:153
  26.5 0.2 stack.9
  26.7 3.1 %convolution_convert_fusion.5 = bf16[64,2048]{1,0:T(8,128)(2,1)S(1)} fusion(bf16[1024,2048]{1,0:T(8,128)(2,1)} %param.38, f32[64,1024]{1,0:T(8,128)S(1)} %copy.210, f32[1024]{0:T(1024)S(1)} %copy-done.14, f32[1024]{0:T(1024)S(1)} %dynamic_slice.18, f32[64]{0:T(128)S(1)} %add_rsqrt_fusion.1, bf16[64,1024]{1,0:T(8,128)(2,1)S(1)} %copy-done.7), kind=kOutput, calls=%fused_computation.7 | convolution fusion | flops 269615104 | bytes 4858112 | tf_op jit(solution)/shard_map/dot_general | solution.py:152
  29.9 0.2 stack.8
  30.2 4.2 %all_to_all.62 = bf16[2,64,2,1024]{3,1,2,0:T(8,128)(2,1)S(1)} all-to-all(bf16[2,64,2,1024]{3,1,2,0:T(8,128)(2,1)S(1)} %maximum_bitcast_fusion), channel_id=1, replica_groups=mesh['ep'=64,'tp'=2] {'tp'}, dimensions={0} | all-to-all | bytes 1048576 | tf_op jit(solution)/shard_map/all_to_all | solution.py:23
  34.5 0.2 fusion.44
  34.7 0.2 dynamic-update-slice.1
  34.9 2.4 all-reduce.1
  37.6 0.7 broadcast_in_dim.33
  38.3 3.4 %all-to-all-start.2 = ((bf16[2,64,1024]{2,1,0:T(8,128)(2,1)}), bf16[2,64,1024]{2,1,0:T(8,128)(2,1)S(1)}, u32[]{:S(2)}, u32[]{:S(2)}) async-start(bf16[2,64,1024]{2,1,0:T(8,128)(2,1)} %broadcast_in_dim.33), calls=%async_computation.2 | async-start | bytes 524288 | tf_op jit(solution)/shard_map/all_to_all | solution.py:29
  41.9 1.4 all-to-all-done.2
  43.3 0.7 copy.244
  44.4 0.2 reduce_window_sum.11
  45.1 1.4 convolution_convert_fusion.3
  46.5 1.2 reshape.203
  47.7 11.5 %all-to-all-start.3 = ((bf16[64,4,2048]{2,1,0:T(4,128)(2,1)}), bf16[64,4,2048]{2,1,0:T(4,128)(2,1)S(1)}, u32[]{:S(2)}, u32[]{:S(2)}) async-start(bf16[64,4,2048]{2,1,0:T(4,128)(2,1)} %reshape.203), calls=%async_computation.3 | async-start | bytes 2097152 | tf_op jit(solution)/shard_map/all_to_all | solution.py:198
  59.3 0.9 constant_dynamic-slice_fusion
  60.2 0.2 fusion.42
  60.6 0.2 convolution_bitcast_fusion
  60.8 17.7 %all-to-all-done.3 = bf16[64,4,2048]{2,1,0:T(4,128)(2,1)S(1)} async-done(((bf16[64,4,2048]{2,1,0:T(4,128)(2,1)}), bf16[64,4,2048]{2,1,0:T(4,128)(2,1)S(1)}, u32[]{:S(2)}, u32[]{:S(2)}) %all-to-all-start.3) | async-done | bytes 1048608 | tf_op jit(solution)/shard_map/all_to_all | solution.py:198
  78.5 0.6 broadcast_in_dim.24
  79.1 3.3 %all-to-all-start.1 = ((f32[2,1,4416]{2,1,0:T(1,128)}), f32[2,1,4416]{2,1,0:T(1,128)S(1)}, u32[]{:S(2)}, u32[]{:S(2)}) async-start(f32[2,1,4416]{2,1,0:T(1,128)} %broadcast_in_dim.24), calls=%async_computation.1 | async-start | bytes 71680 | tf_op jit(solution)/shard_map/all_to_all | solution.py:29
  82.4 1.1 reshape.204
  83.5 3.4 %fusion.3 = f32[256,512]{1,0:T(8,128)} fusion(bf16[256,2048]{1,0:T(8,128)(2,1)} %reshape.204, bf16[1,2048,512]{2,1,0:T(8,128)(2,1)} %param.44), kind=kOutput, calls=%fused_computation.11 | convolution fusion | flops 536870912 | bytes 3670016 | tf_op jit(solution)/shard_map/dot_general | solution.py:202
  86.9 3.3 %convolution_convert_fusion.2 = bf16[256,2048]{1,0:T(8,128)(2,1)S(1)} fusion(bf16[1,512,2048]{2,1,0:T(8,128)(2,1)S(1)} %copy-done, bf16[256,2048]{1,0:T(8,128)(2,1)} %reshape.204, bf16[1,2048,512]{2,1,0:T(8,128)(2,1)} %param.45, f32[256,512]{1,0:T(8,128)} %fusion.3), kind=kOutput, calls=%fused_computation.4 | convolution fusion | flops 1075052544 | bytes 6815744 | tf_op jit(solution)/shard_map/dot_general | solution.py:205
  90.2 0.2 broadcast_in_dim.34
  90.5 6.3 %all_to_all.60 = bf16[2,256,2048]{2,1,0:T(8,128)(2,1)} all-to-all(bf16[2,256,2048]{2,1,0:T(8,128)(2,1)S(1)} %broadcast_in_dim.34), channel_id=1, replica_groups=mesh['ep'=64,'tp'=2] {'tp'}, dimensions={0} | all-to-all | bytes 4194304 | tf_op jit(solution)/shard_map/all_to_all | solution.py:29
  96.8 4.3 %stack.11 = bf16[64,64,1024]{2,1,0:T(8,128)(2,1)} broadcast(bf16[64,1024]{1,0:T(8,128)(2,1)S(1)} %fusion.40), dimensions={1,2} | broadcast | bytes 8519680 | tf_op jit(solution)/shard_map/stack | solution.py:215
  101.1 5.9 %all-to-all-start.6 = ((bf16[64,64,1024]{2,1,0:T(8,128)(2,1)}), bf16[64,64,1024]{2,1,0:T(8,128)(2,1)}, u32[]{:S(2)}, u32[]{:S(2)}) async-start(bf16[64,64,1024]{2,1,0:T(8,128)(2,1)} %stack.11), calls=%async_computation.6 | async-start | bytes 16777216 | tf_op jit(solution)/shard_map/all_to_all | solution.py:215
  107.0 3.9 %copy.229 = f32[64,64,64]{2,1,0:T(8,128)} copy(f32[64,64,64]{0,2,1:T(8,128)} %copy-done.4) | data formatting | bytes 2097152
  110.9 2.7 copy.230
  114.3 0.2 select_reduce_fusion.1
  114.7 2.0 convert_reduce_fusion
  116.8 1.0 reshape.205
  117.8 107.2 %all-to-all-done.6 = bf16[64,64,1024]{2,1,0:T(8,128)(2,1)} async-done(((bf16[64,64,1024]{2,1,0:T(8,128)(2,1)}), bf16[64,64,1024]{2,1,0:T(8,128)(2,1)}, u32[]{:S(2)}, u32[]{:S(2)}) %all-to-all-start.6) | async-done | bytes 8388640 | tf_op jit(solution)/shard_map/all_to_all | solution.py:215
  225.0 6.0 %convolution_convert_fusion = bf16[4096,32]{0,1:T(8,128)(2,1)S(1)} fusion(bf16[4096,1024]{1,0:T(8,128)(2,1)} %bitcast.16, bf16[1024,32]{0,1:T(8,128)(2,1)S(1)} %copy-done.12), kind=kOutput, calls=%fused_computation.1 | convolution fusion | flops 268566528 | bytes 8716288 | tf_op jit(solution)/shard_map/dot_general | solution.py:99
  231.0 5.9 %convolution_convert_fusion.1 = bf16[4096,32]{0,1:T(8,128)(2,1)S(1)} fusion(bf16[4096,1024]{1,0:T(8,128)(2,1)} %bitcast.16, bf16[1024,32]{0,1:T(8,128)(2,1)S(1)} %copy-done.13), kind=kOutput, calls=%fused_computation.2 | convolution fusion | flops 268566528 | bytes 8716288 | tf_op jit(solution)/shard_map/dot_general | solution.py:98
  237.1 4.6 %all_to_all.61 = bf16[2,4096,64]{1,2,0:T(8,128)(2,1)S(1)} all-to-all(bf16[2,4096,64]{1,2,0:T(8,128)(2,1)S(1)} %broadcast_in_dim.35), channel_id=1, replica_groups=mesh['ep'=64,'tp'=2] {'tp'}, dimensions={0} | all-to-all | bytes 2097152 | tf_op jit(solution)/shard_map/all_to_all | solution.py:29
  241.7 16.9 %all-to-all-start.5 = ((bf16[64,4,1024]{2,1,0:T(4,128)(2,1)}), bf16[64,4,1024]{2,1,0:T(4,128)(2,1)S(1)}, u32[]{:S(2)}, u32[]{:S(2)}) async-start(bf16[64,4,1024]{2,1,0:T(4,128)(2,1)} %reshape.205), calls=%async_computation.5 | async-start | bytes 1048576 | tf_op jit(solution)/shard_map/all_to_all | solution.py:209
  259.0 0.5 all_to_all.47
  259.5 0.3 copy.246
  259.9 1.0 reshape.234
  260.9 11.4 %all-to-all-done.5 = bf16[64,4,1024]{2,1,0:T(4,128)(2,1)S(1)} async-done(((bf16[64,4,1024]{2,1,0:T(4,128)(2,1)}), bf16[64,4,1024]{2,1,0:T(4,128)(2,1)S(1)}, u32[]{:S(2)}, u32[]{:S(2)}) %all-to-all-start.5) | async-done | bytes 524320 | tf_op jit(solution)/shard_map/all_to_all | solution.py:209
  272.3 5.0 %all-to-all-start.8 = ((bf16[64,2,1024]{2,1,0:T(2,128)(2,1)}), bf16[64,2,1024]{2,1,0:T(2,128)(2,1)S(1)}, u32[]{:S(2)}, u32[]{:S(2)}) async-start(bf16[64,2,1024]{2,1,0:T(2,128)(2,1)} %reshape.234), calls=%async_computation.8 | async-start | bytes 524288 | tf_op jit(solution)/shard_map/all_to_all | solution.py:225
  277.4 0.9 gather_fusion
  278.3 0.3 reshape.209
  278.6 0.7 multiply_reduce_fusion
  279.3 8.3 %all-to-all-done.8 = bf16[64,2,1024]{2,1,0:T(2,128)(2,1)S(1)} async-done(((bf16[64,2,1024]{2,1,0:T(2,128)(2,1)}), bf16[64,2,1024]{2,1,0:T(2,128)(2,1)S(1)}, u32[]{:S(2)}, u32[]{:S(2)}) %all-to-all-start.8) | async-done | bytes 262176 | tf_op jit(solution)/shard_map/all_to_all | solution.py:225
  287.6 0.3 reshape.235
  288.0 3.9 %fusion.12 = bf16[64,1024]{1,0:T(8,128)(2,1)} fusion(bf16[64,2048]{0,1:T(8,128)(2,1)S(1)} %bitcast.78, bf16[2048,1024]{1,0:T(8,128)(2,1)} %param.49, f32[64,1024]{1,0:T(8,128)S(1)} %multiply_reduce_fusion, bf16[64,1024]{1,0:T(8,128)(2,1)S(1)} %get-tuple-element.28, f32[64]{0:T(128)S(1)} %fusion.73), kind=kOutput, calls=%fused_computation.21 | convolution fusion | flops 268763136 | bytes 4980992 | tf_op jit(solution)/shard_map/dot_general | solution.py:226
  (98 shorter events, 3.5 us)
Async XLA Ops:
  0.6 86.3 %copy-start = (bf16[1,512,2048]{2,1,0:T(8,128)(2,1)S(1)}, bf16[1,512,2048]{2,1,0:T(8,128)(2,1)}, u32[]{:S(2)}) copy-start(bf16[1,512,2048]{2,1,0:T(8,128)(2,1)} %param.46) | copy-start | bytes 6291460
  4.1 3.5 %copy-start.7 = (bf16[64,1024]{1,0:T(8,128)(2,1)S(1)}, bf16[64,1024]{1,0:T(8,128)(2,1)}, u32[]{:S(2)}) copy-start(bf16[64,1024]{1,0:T(8,128)(2,1)} %param.25) | copy-start | bytes 393220
  4.1 3.6 %copy-start.20 = (u32[128]{0:T(128)S(1)}, u32[128]{0:T(128)}, u32[]{:S(2)}) copy-start(u32[128]{0:T(128)} %constant.69) | copy-start | bytes 1540
  4.1 7.6 %copy-start.17 = (f32[2048]{0:T(1024)S(1)}, f32[2048]{0:T(1024)}, u32[]{:S(2)}) copy-start(f32[2048]{0:T(1024)} %param.28) | copy-start | bytes 24580
  4.1 9.5 %copy-start.19 = (f32[64]{0:T(128)S(1)}, f32[64]{0:T(128)}, u32[]{:S(2)}) copy-start(f32[64]{0:T(128)} %param.32) | copy-start | bytes 772
  4.1 10.5 %copy-start.8 = (f32[64,64,16]{1,2,0:T(8,128)S(1)}, f32[64,64,16]{1,2,0:T(8,128)}, u32[]{:S(2)}) copy-start(f32[64,64,16]{1,2,0:T(8,128)} %param.34) | copy-start | bytes 786436
  4.1 10.5 %copy-start.9 = (f32[64,64,16]{1,2,0:T(8,128)S(1)}, f32[64,64,16]{1,2,0:T(8,128)}, u32[]{:S(2)}) copy-start(f32[64,64,16]{1,2,0:T(8,128)} %param.33) | copy-start | bytes 786436
  14.7 4.0 %copy-start.5 = (f32[64,64,64]{0,2,1:T(8,128)S(1)}, f32[64,64,64]{0,2,1:T(8,128)}, u32[]{:S(2)}) copy-start(f32[64,64,64]{0,2,1:T(8,128)} %copy.204) | copy-start | bytes 3145732
  14.7 4.0 %copy-start.6 = (f32[64,64,64]{0,2,1:T(8,128)S(1)}, f32[64,64,64]{0,2,1:T(8,128)}, u32[]{:S(2)}) copy-start(f32[64,64,64]{0,2,1:T(8,128)} %copy.203) | copy-start | bytes 3145732
  18.7 2.5 copy-start.4
  18.7 2.5 copy-start.11
  21.2 1.9 copy-start.2
  21.2 1.4 copy-start.10
  22.6 0.7 copy-start.14
  30.1 7.3 %copy-start.18 = (f32[2048]{0:T(1024)S(1)}, f32[2048]{0:T(1024)}, u32[]{:S(2)}) copy-start(f32[2048]{0:T(1024)} %param.29) | copy-start | bytes 24580
  30.2 11.6 %copy-start.15 = (s32[64,2]{0,1:T(2,128)S(1)}, s32[64,2]{0,1:T(2,128)}, u32[]{:S(2)}) copy-start(s32[64,2]{0,1:T(2,128)} %param.43) | copy-start | bytes 1540
  38.3 5.0 %all-to-all-start.2 = ((bf16[2,64,1024]{2,1,0:T(8,128)(2,1)}), bf16[2,64,1024]{2,1,0:T(8,128)(2,1)S(1)}, u32[]{:S(2)}, u32[]{:S(2)}) async-start(bf16[2,64,1024]{2,1,0:T(8,128)(2,1)} %broadcast_in_dim.33), calls=%async_computation.2 | async-start | bytes 524288 | tf_op jit(solution)/shard_map/all_to_all | solution.py:29
  46.5 12.8 %copy-start.16 = (bf16[2048,4]{0,1:T(4,128)(2,1)S(1)}, bf16[2048,4]{0,1:T(4,128)(2,1)}, u32[]{:S(2)}) copy-start(bf16[2048,4]{0,1:T(4,128)(2,1)} %param.40) | copy-start | bytes 49156
  46.5 14.1 %dynamic-slice-start = ((f32[2048]{0:T(1024)}, s32[]{:T(128)}), f32[1024]{0:T(1024)S(1)}, s32[]{:S(2)}) async-start(f32[2048]{0:T(1024)} %param.42, s32[]{:T(128)} %select_n.31), calls=%async_computation.9 | async-start | bytes 8704 | tf_op jit(solution)/shard_map/dynamic_slice | solution.py:135
  47.7 30.7 %all-to-all-start.3 = ((bf16[64,4,2048]{2,1,0:T(4,128)(2,1)}), bf16[64,4,2048]{2,1,0:T(4,128)(2,1)S(1)}, u32[]{:S(2)}, u32[]{:S(2)}) async-start(bf16[64,4,2048]{2,1,0:T(4,128)(2,1)} %reshape.203), calls=%async_computation.3 | async-start | bytes 2097152 | tf_op jit(solution)/shard_map/all_to_all | solution.py:198
  79.1 11.1 %all-to-all-start.1 = ((f32[2,1,4416]{2,1,0:T(1,128)}), f32[2,1,4416]{2,1,0:T(1,128)S(1)}, u32[]{:S(2)}, u32[]{:S(2)}) async-start(f32[2,1,4416]{2,1,0:T(1,128)} %broadcast_in_dim.24), calls=%async_computation.1 | async-start | bytes 71680 | tf_op jit(solution)/shard_map/all_to_all | solution.py:29
  101.1 124.0 %all-to-all-start.6 = ((bf16[64,64,1024]{2,1,0:T(8,128)(2,1)}), bf16[64,64,1024]{2,1,0:T(8,128)(2,1)}, u32[]{:S(2)}, u32[]{:S(2)}) async-start(bf16[64,64,1024]{2,1,0:T(8,128)(2,1)} %stack.11), calls=%async_computation.6 | async-start | bytes 16777216 | tf_op jit(solution)/shard_map/all_to_all | solution.py:215
  107.0 3.9 %copy-start.3 = (f32[64,64,64]{0,2,1:T(8,128)S(1)}, f32[64,64,64]{0,2,1:T(8,128)}, u32[]{:S(2)}) copy-start(f32[64,64,64]{0,2,1:T(8,128)} %copy-done.2) | copy-start | bytes 3145732
  114.7 110.3 %copy-start.12 = (bf16[1024,32]{0,1:T(8,128)(2,1)S(1)}, bf16[1024,32]{0,1:T(8,128)(2,1)}, u32[]{:S(2)}) copy-start(bf16[1024,32]{0,1:T(8,128)(2,1)} %param.48) | copy-start | bytes 196612
  225.0 6.0 %copy-start.13 = (bf16[1024,32]{0,1:T(8,128)(2,1)S(1)}, bf16[1024,32]{0,1:T(8,128)(2,1)}, u32[]{:S(2)}) copy-start(bf16[1024,32]{0,1:T(8,128)(2,1)} %param.47) | copy-start | bytes 196612
  241.7 30.6 %all-to-all-start.5 = ((bf16[64,4,1024]{2,1,0:T(4,128)(2,1)}), bf16[64,4,1024]{2,1,0:T(4,128)(2,1)S(1)}, u32[]{:S(2)}, u32[]{:S(2)}) async-start(bf16[64,4,1024]{2,1,0:T(4,128)(2,1)} %reshape.205), calls=%async_computation.5 | async-start | bytes 1048576 | tf_op jit(solution)/shard_map/all_to_all | solution.py:209
  272.3 15.3 %all-to-all-start.8 = ((bf16[64,2,1024]{2,1,0:T(2,128)(2,1)}), bf16[64,2,1024]{2,1,0:T(2,128)(2,1)S(1)}, u32[]{:S(2)}, u32[]{:S(2)}) async-start(bf16[64,2,1024]{2,1,0:T(2,128)(2,1)} %reshape.234), calls=%async_computation.8 | async-start | bytes 524288 | tf_op jit(solution)/shard_map/all_to_all | solution.py:225
  288.0 3.9 %copy-start.1 = (bf16[1,512,2048]{2,1,0:T(8,128)(2,1)S(1)}, bf16[1,512,2048]{2,1,0:T(8,128)(2,1)}, u32[]{:S(2)}) copy-start(bf16[1,512,2048]{2,1,0:T(8,128)(2,1)} %param.46) | copy-start | bytes 6291460
